TPU v7x, 32 devices: a whole 2x2x4 slice. The times are simulated.
32 devices in a mesh: sp: 16 (over z, y, x), tp: 2 (over core).
Axes of the slice: x: 2, y: 2, z: 4, core: 2. Of those that a mesh axis runs over, the one named last changes fastest.
Arguments:
- residual: bfloat16 [3072, 2048], P(('sp', 'tp')), may hold values from -6 to 6
- queries_narrow: bfloat16 [3072, 512], P('sp', 'tp'), may hold values from -24 to 24
- keys_narrow: bfloat16 [3072, 512], P('sp', 'tp'), may hold values from -24 to 24
- values_narrow: bfloat16 [3072, 512], P('sp', 'tp'), may hold values from -6 to 6
- queries_broad: bfloat16 [3072, 512], P('sp', 'tp'), may hold values from -24 to 24
- keys_broad: bfloat16 [3072, 512], P('sp', 'tp'), may hold values from -24 to 24
- values_broad: bfloat16 [3072, 512], P('sp', 'tp'), may hold values from -6 to 6
- gates_narrow: float32 [3072, 16], P('sp', 'tp'), may hold values from -3072 to 0, as said below
- gates_broad: float32 [3072, 8], P('sp', 'tp'), may hold values from -3072 to 0, as said below
- project_narrow: bfloat16 [512, 2048], P('tp'), may hold values from -0.5 to 0.5
- project_broad: bfloat16 [512, 2048], P('tp'), may hold values from -0.5 to 0.5
- norm_gain: float32 [2048], replicated, may hold values from 0.1 to 1.9
- up_weight: bfloat16 [2048, 8192], P('sp', 'tp'), may hold values from -0.125 to 0.125
- down_weight: bfloat16 [8192, 2048], P('tp', 'sp'), may hold values from -0.0625 to 0.0625
Outputs:
- layer_out: bfloat16 [3072, 2048], P(('sp', 'tp'))
Inputs may be any that keep to these rules, and one draw needn't show every extreme that they name: `gates_narrow`: each head's cumulative log gate never rises from one position to the next. `gates_broad`: each head's cumulative log gate never rises from one position to the next.
All inputs are finite; a program needn't handle non-finite values.
Results may differ from a plain program's by a relative error of at most 0.018.
Values may be sent and summed in bfloat16 or wider, within the bound.
A program may use at most 128 MiB of HBM per device.

v0:
```python
import jax
import jax.numpy as jnp
from jax import lax
from jax.sharding import PartitionSpec as P

A_DIM = 32
B_DIM = 64


def group_update(state, queries, keys, values, query_gates, key_gates, allowed, head_size):
    peak, total, summed = state
    query_count = queries.shape[0]
    key_count = keys.shape[0]
    heads = queries.shape[1] // head_size
    scores = jnp.einsum(
        "qhd,khd->hqk",
        queries.reshape(query_count, heads, head_size),
        keys.reshape(key_count, heads, head_size),
        preferred_element_type=jnp.float32,
    ) * head_size ** (-0.5)
    scores = scores + query_gates.T[:, :, None] - key_gates.T[:, None, :]
    scores = jnp.where(allowed[None], scores, -1e30)
    new_peak = jnp.maximum(peak, jnp.max(scores, axis=-1))
    weights = jnp.exp(scores - new_peak[..., None]) * allowed[None].astype(jnp.float32)
    total = jnp.sum(weights, axis=-1)
    summed = jnp.einsum(
        "hqk,khd->hqd",
        weights.astype(jnp.bfloat16),
        values.reshape(key_count, heads, head_size),
        preferred_element_type=jnp.float32,
    )
    return (new_peak, total, summed)


def empty_state(query_count, heads, head_size):
    return (
        jnp.full((heads, query_count), -1e30, jnp.float32),
        jnp.zeros((heads, query_count), jnp.float32),
        jnp.zeros((heads, query_count, head_size), jnp.float32),
    )


def finish_group(state, head_size):
    peak, total, summed = state
    result = summed / total[..., None]
    return (
        result.transpose(1, 0, 2)
        .reshape(result.shape[1], result.shape[0] * head_size)
        .astype(jnp.bfloat16)
    )


def rms_scaled(mixed, norm_gain):
    mixed_wide = mixed.astype(jnp.float32)
    scale = lax.rsqrt(jnp.mean(mixed_wide * mixed_wide, axis=-1, keepdims=True) + 1e-06)
    return (mixed_wide * scale * norm_gain).astype(jnp.bfloat16)


def local(
    residual,
    queries_narrow,
    keys_narrow,
    values_narrow,
    queries_broad,
    keys_broad,
    values_broad,
    gates_narrow,
    gates_broad,
    project_narrow,
    project_broad,
    norm_gain,
    up_weight,
    down_weight,
):
    local_count = queries_narrow.shape[0]
    table_narrow, table_broad = (
        lax.all_gather(gates_narrow, "sp", axis=0, tiled=True),
        lax.all_gather(gates_broad, "sp", axis=0, tiled=True),
    )
    query_pos = lax.axis_index("sp") * local_count + jnp.arange(local_count, dtype=jnp.int32)
    initial = (
        empty_state(local_count, queries_narrow.shape[1] // A_DIM, A_DIM),
        empty_state(local_count, queries_broad.shape[1] // B_DIM, B_DIM),
    )
    piece_keys_narrow = lax.all_gather(keys_narrow, "sp", axis=0, tiled=True)
    piece_values_narrow = lax.all_gather(values_narrow, "sp", axis=0, tiled=True)
    piece_keys_broad = lax.all_gather(keys_broad, "sp", axis=0, tiled=True)
    piece_values_broad = lax.all_gather(values_broad, "sp", axis=0, tiled=True)
    piece_count = piece_keys_narrow.shape[0]
    key_pos = jnp.arange(piece_count, dtype=jnp.int32)
    allowed = key_pos[None, :] <= query_pos[:, None]
    state_narrow = group_update(
        initial[0],
        queries_narrow,
        piece_keys_narrow,
        piece_values_narrow,
        gates_narrow,
        table_narrow,
        allowed,
        A_DIM,
    )
    state_broad = group_update(
        initial[1],
        queries_broad,
        piece_keys_broad,
        piece_values_broad,
        gates_broad,
        table_broad,
        allowed,
        B_DIM,
    )
    attended_narrow = finish_group(state_narrow, A_DIM)
    attended_broad = finish_group(state_broad, B_DIM)
    projected = lax.psum_scatter(
        (
            jnp.dot(attended_narrow, project_narrow, preferred_element_type=jnp.float32)
            + jnp.dot(attended_broad, project_broad, preferred_element_type=jnp.float32)
        ).astype(jnp.bfloat16),
        "tp",
        scatter_dimension=0,
        tiled=True,
    ).astype(jnp.float32)
    mixed = (residual.astype(jnp.float32) + projected).astype(jnp.bfloat16)
    features = lax.all_gather(rms_scaled(mixed, norm_gain), "tp", axis=0, tiled=True)
    up_total = jnp.dot(
        features,
        lax.all_gather(up_weight, "sp", axis=0, tiled=True),
        preferred_element_type=jnp.float32,
    )
    hidden = jnp.square(jax.nn.relu(up_total)).astype(jnp.bfloat16)
    down_term = jnp.dot(
        hidden,
        lax.all_gather(down_weight, "sp", axis=1, tiled=True),
        preferred_element_type=jnp.float32,
    )
    summed_rows = lax.psum_scatter(
        down_term.astype(jnp.bfloat16), "tp", scatter_dimension=0, tiled=True
    ).astype(jnp.float32)
    return (mixed.astype(jnp.float32) + summed_rows).astype(jnp.bfloat16)


def solution(mesh):
    return jax.shard_map(
        local,
        mesh=mesh,
        in_specs=(
            P(("sp", "tp"), None),
            P("sp", "tp"),
            P("sp", "tp"),
            P("sp", "tp"),
            P("sp", "tp"),
            P("sp", "tp"),
            P("sp", "tp"),
            P("sp", "tp"),
            P("sp", "tp"),
            P("tp", None),
            P("tp", None),
            P(),
            P("sp", "tp"),
            P("tp", "sp"),
        ),
        out_specs=P(("sp", "tp"), None),
        check_vma=False,
    )
```

profile of v0, /device:TPU:0, one launch (start us, length us, event | category | flops | bytes accessed | tf_op | source)
XLA Modules:
  0.0 742.3 jit_solution(3498710460941625432)
XLA Ops:
  6.5 0.7 all-gather.9.cloned.1.call-update
  7.3 0.0 all-gather.13.cloned.1.call-start
  7.3 0.7 all-gather.13.cloned.1.call-update
  8.0 0.0 all-gather.11.cloned.1.call-start
  8.1 0.7 all-gather.11.cloned.1.call-update
  8.7 0.0 all-gather.15.cloned.1.call-start
  8.8 0.5 all-gather.15.cloned.1.call-update
  9.3 0.0 reduce-scatter.3.cloned.1.call-start
  9.4 1.3 iota_compare_fusion
  10.7 43.5 %all-gather = f32[16,192,8]{1,2,0:T(8,128)S(1)} all-gather(f32[1,192,8]{1,2,0:T(8,128)} %bitcast.59), channel_id=1, replica_groups=mesh['sp'=16,'tp'=2] {'sp'}, dimensions={0}, use_global_device_ids=true | all-gather | bytes 104448 | tf_op jit(solution)/shard_map/all_gather | solution.py:77
  54.3 0.7 reshape.92
  55.0 1.7 copy.29
  56.7 36.3 %all-gather.1 = f32[16,192,4]{1,2,0:T(4,128)S(1)} all-gather(f32[1,192,4]{1,2,0:T(4,128)} %bitcast.65), channel_id=1, replica_groups=mesh['sp'=16,'tp'=2] {'sp'}, dimensions={0}, use_global_device_ids=true | all-gather | bytes 52224 | tf_op jit(solution)/shard_map/all_gather | solution.py:78
  93.0 0.1 reshape.94
  93.1 1.6 copy.33
  94.7 2.6 copy.30
  97.3 7.4 fusion.2
  104.8 6.4 copy-done.4
  111.2 0.4 copy-done.14
  111.5 8.6 %fusion = f32[8,192]{1,0:T(8,128)} fusion(f32[8,192,3072]{2,1,0:T(8,128)S(1)} %get-tuple-element.8, f32[192,3072]{1,0:T(8,128)S(1)} %get-tuple-element.6, f32[8,192]{1,0:T(8,128)S(1)} %broadcast_maximum_fusion, f32[8,3072]{1,0:T(8,128)S(1)} %bitcast.53, f32[8,192]{1,0:T(8,128)S(1)} %bitcast.61, pred[192,3072]{1,0:T(8,128)(4,1)S(1)} %copy-done.8), kind=kLoop, calls=%fused_computation.2 | loop fusion | flops 33028608 | bytes 21940224 | tf_op jit(solution)/shard_map/reduce_sum | solution.py:25
  120.2 10.4 %all-gather.13.cloned.1.call-done = bf16[3072,256]{1,0:T(8,128)(2,1)} async-done(((bf16[192,256]{1,0:T(8,128)(2,1)}), bf16[3072,256]{1,0:T(8,128)(2,1)}) %all-gather.13.cloned.1.call-update) | async-done | bytes 1572880 | tf_op jit(solution)/shard_map/all_gather | solution.py:87
  130.6 2.6 copy.34
  133.2 8.0 %fusion.41 = (f32[4,192]{1,0:T(4,128)S(1)}, f32[4,192,3072]{2,1,0:T(8,128)}) fusion(f32[4,3072]{1,0:T(4,128)S(1)} %bitcast.58, f32[4,192]{1,0:T(4,128)} %bitcast.66, bf16[192,4,64]{0,2,1:T(8,128)(2,1)} %bitcast.55, bf16[3072,4,64]{0,2,1:T(8,128)(2,1)} %bitcast.49, pred[192,3072]{1,0:T(8,128)(4,1)} %get-tuple-element.5), kind=kOutput, calls=%fused_computation.43 | convolution fusion | flops 313785600 | bytes 11753472 | tf_op jit(solution)/shard_map/qhd,khd->hqk/dot_general | solution.py:15
  141.1 48.9 %all-gather.11.cloned.1.call-done = bf16[3072,256]{1,0:T(8,128)(2,1)} async-done(((bf16[192,256]{1,0:T(8,128)(2,1)}), bf16[3072,256]{1,0:T(8,128)(2,1)}) %all-gather.11.cloned.1.call-update) | async-done | bytes 1572880 | tf_op jit(solution)/shard_map/all_gather | solution.py:86
  190.1 2.7 copy.32
  192.8 11.0 %fusion.24 = bf16[192,8,32]{0,2,1:T(8,128)(2,1)S(1)} fusion(bf16[3072,8,32]{0,2,1:T(8,128)(2,1)} %bitcast.48, f32[8,192,3072]{2,1,0:T(8,128)} %copy-done.4, f32[192,3072]{1,0:T(8,128)} %copy-done.2, f32[8,192]{1,0:T(8,128)S(1)} %copy-done.15, f32[8,3072]{1,0:T(8,128)S(1)} %bitcast.54, f32[8,192]{1,0:T(8,128)S(1)} %bitcast.62, ...), kind=kOutput, calls=%fused_computation.27 | convolution fusion | flops 335118336 | bytes 23611392 | tf_op jit(solution)/shard_map/hqk,khd->hqd/dot_general | solution.py:26
  203.8 1.6 fusion.42
  205.4 1.8 fusion.6
  207.3 42.1 %all-gather.15.cloned.1.call-done = bf16[3072,256]{1,0:T(8,128)(2,1)} async-done(((bf16[192,256]{1,0:T(8,128)(2,1)}), bf16[3072,256]{1,0:T(8,128)(2,1)}) %all-gather.15.cloned.1.call-update) | async-done | bytes 1572880 | tf_op jit(solution)/shard_map/all_gather | solution.py:88
  249.4 2.6 copy.36
  252.0 6.7 fusion.30
  258.8 1.3 fusion.14
  260.1 0.0 reduce-scatter.3.cloned.1.call-update
  260.1 0.0 all-gather.17.cloned.1.call-start
  260.2 0.5 all-gather.17.cloned.1.call-update
  260.7 0.0 all-gather.19.cloned.1.call-start
  260.7 0.7 all-gather.19.cloned.1.call-update
  261.4 0.0 reduce-scatter.5.cloned.1.call-start
  261.5 5.7 reduce-scatter.3.cloned.1.call-done
  267.1 1.2 fusion.33
  268.4 1.2 fusion.35
  269.6 2.4 all_gather.33
  271.9 190.0 %all-gather.17.cloned.1.call-done = bf16[2048,4096]{1,0:T(8,128)(2,1)} async-done(((bf16[128,4096]{1,0:T(8,128)(2,1)}), bf16[2048,4096]{1,0:T(8,128)(2,1)}) %all-gather.17.cloned.1.call-update) | async-done | bytes 16777232 | tf_op jit(solution)/shard_map/all_gather | solution.py:127
  461.9 250.0 %all-gather.19.cloned.1.call-done = bf16[4096,2048]{1,0:T(8,128)(2,1)} async-done(((bf16[4096,128]{1,0:T(8,128)(2,1)}), bf16[4096,2048]{1,0:T(8,128)(2,1)}) %all-gather.19.cloned.1.call-update) | async-done | bytes 16777232 | tf_op jit(solution)/shard_map/all_gather | solution.py:133
  711.9 15.1 %convolution_convert_fusion = bf16[192,2048]{1,0:T(8,128)(2,1)} fusion(bf16[4096,2048]{1,0:T(8,128)(2,1)} %all-gather.19.cloned.1.call-done, bf16[192,2048]{1,0:T(8,128)(2,1)S(1)} %all_gather.33, bf16[2048,4096]{1,0:T(8,128)(2,1)} %all-gather.17.cloned.1.call-done), kind=kOutput, calls=%fused_computation.18 | convolution fusion | flops 6445203456 | bytes 35127296 | tf_op jit(solution)/shard_map/dot_general | solution.py:131
  727.0 0.0 reduce-scatter.5.cloned.1.call-update
  727.0 6.5 reduce-scatter.5.cloned.1.call-done
  733.5 1.9 fusion.36
  (49 shorter events, 0.2 us)
Async XLA Ops:
  6.5 197.3 %copy-start = (bf16[256,2048]{1,0:T(8,128)(2,1)S(1)}, bf16[256,2048]{1,0:T(8,128)(2,1)}, u32[]{:S(2)}) copy-start(bf16[256,2048]{1,0:T(8,128)(2,1)} %param.23) | copy-start | bytes 3145732
  6.5 88.2 %all-gather.9.cloned.1.call-start = ((), (), s32[]{:S(2)}) async-start(), calls=%async_computation.2 | async-start | bytes 1671168 | tf_op jit(solution)/shard_map/all_gather | solution.py:85
  7.3 123.3 %all-gather.13.cloned.1.call-start = ((), (), s32[]{:S(2)}) async-start(), calls=%async_computation.4 | async-start | bytes 1671168 | tf_op jit(solution)/shard_map/all_gather | solution.py:87
  8.0 182.0 %all-gather.11.cloned.1.call-start = ((), (), s32[]{:S(2)}) async-start(), calls=%async_computation.3 | async-start | bytes 1671168 | tf_op jit(solution)/shard_map/all_gather | solution.py:86
  8.7 240.7 %all-gather.15.cloned.1.call-start = ((), (), s32[]{:S(2)}) async-start(), calls=%async_computation.5 | async-start | bytes 1671168 | tf_op jit(solution)/shard_map/all_gather | solution.py:88
  9.3 257.8 %reduce-scatter.3.cloned.1.call-start = ((), (), s32[]{:S(2)}) async-start(), calls=%async_computation.6 | async-start | bytes 1179648 | tf_op jit(solution)/shard_map/reduce_scatter | solution.py:114
  10.7 94.0 %copy-start.2 = (f32[192,3072]{1,0:T(8,128)}, f32[192,3072]{1,0:T(8,128)S(1)}, u32[]{:S(2)}) copy-start(f32[192,3072]{1,0:T(8,128)S(1)} %get-tuple-element.6) | copy-start | bytes 7077892
  97.3 14.2 %copy-start.8 = (pred[192,3072]{1,0:T(8,128)(4,1)S(1)}, pred[192,3072]{1,0:T(8,128)(4,1)}, u32[]{:S(2)}) copy-start(pred[192,3072]{1,0:T(8,128)(4,1)} %get-tuple-element.5) | copy-start | bytes 1769476
  97.3 14.2 %copy-start.11 = (f32[3072,8]{0,1:T(8,128)S(1)}, f32[3072,8]{0,1:T(8,128)}, u32[]{:S(2)}) copy-start(f32[3072,8]{0,1:T(8,128)} %reshape.92) | copy-start | bytes 294916
  97.3 14.2 %copy-start.12 = (f32[192,8]{0,1:T(8,128)S(1)}, f32[192,8]{0,1:T(8,128)}, u32[]{:S(2)}) copy-start(f32[192,8]{0,1:T(8,128)} %param.21) | copy-start | bytes 18436
  104.7 6.4 copy-start.4
  104.7 6.8 copy-start.14
  133.2 59.6 %copy-start.9 = (pred[192,3072]{1,0:T(8,128)(4,1)S(1)}, pred[192,3072]{1,0:T(8,128)(4,1)}, u32[]{:S(2)}) copy-start(pred[192,3072]{1,0:T(8,128)(4,1)} %get-tuple-element.5) | copy-start | bytes 1769476
  133.2 59.6 %copy-start.13 = (f32[192,8]{0,1:T(8,128)S(1)}, f32[192,8]{0,1:T(8,128)}, u32[]{:S(2)}) copy-start(f32[192,8]{0,1:T(8,128)} %param.21) | copy-start | bytes 18436
  133.2 59.6 %copy-start.15 = (f32[8,192]{1,0:T(8,128)S(1)}, f32[8,192]{1,0:T(8,128)}, u32[]{:S(2)}) copy-start(f32[8,192]{1,0:T(8,128)} %copy-done.14) | copy-start | bytes 18436
  133.2 59.6 %copy-start.17 = (f32[8,192]{1,0:T(8,128)S(1)}, f32[8,192]{1,0:T(8,128)}, u32[]{:S(2)}) copy-start(f32[8,192]{1,0:T(8,128)} %fusion) | copy-start | bytes 18436
  190.0 15.4 %slice-start = ((s8[9437184]{0:T(1024)(128)(4,1)}), s8[1048576]{0:T(1024)(128)(4,1)S(1)}, s32[]{:S(2)}) async-start(s8[9437184]{0:T(1024)(128)(4,1)} %bitcast.45), calls=%async_computation.10 | async-start | bytes 2097152
  192.8 12.6 %slice-start.1 = ((s8[9437184]{0:T(1024)(128)(4,1)}), s8[4194304]{0:T(1024)(128)(4,1)S(1)}, s32[]{:S(2)}) async-start(s8[9437184]{0:T(1024)(128)(4,1)} %bitcast.45), calls=%async_computation.11 | async-start | bytes 8388608
  192.8 12.6 %slice-start.2 = ((s8[9437184]{0:T(1024)(128)(4,1)}), s8[4194304]{0:T(1024)(128)(4,1)S(1)}, s32[]{:S(2)}) async-start(s8[9437184]{0:T(1024)(128)(4,1)} %bitcast.45), calls=%async_computation.12 | async-start | bytes 8388608
  192.8 12.6 %copy-start.3 = (f32[192,3072]{1,0:T(8,128)S(1)}, f32[192,3072]{1,0:T(8,128)}, u32[]{:S(2)}) copy-start(f32[192,3072]{1,0:T(8,128)} %copy-done.2) | copy-start | bytes 7077892
  207.3 51.5 %copy-start.5 = (f32[192,2048]{1,0:T(8,128)S(1)}, f32[192,2048]{1,0:T(8,128)}, u32[]{:S(2)}) copy-start(f32[192,2048]{1,0:T(8,128)} %fusion.42) | copy-start | bytes 4718596
  207.3 51.5 %copy-start.10 = (bf16[256,2048]{1,0:T(8,128)(2,1)S(1)}, bf16[256,2048]{1,0:T(8,128)(2,1)}, u32[]{:S(2)}) copy-start(bf16[256,2048]{1,0:T(8,128)(2,1)} %param.24) | copy-start | bytes 3145732
  252.0 15.1 %copy-start.6 = (bf16[96,2048]{1,0:T(8,128)(2,1)S(1)}, bf16[96,2048]{1,0:T(8,128)(2,1)}, u32[]{:S(2)}) copy-start(bf16[96,2048]{1,0:T(8,128)(2,1)} %param.14) | copy-start | bytes 1179652
  252.0 16.4 %copy-start.16 = (f32[2048]{0:T(1024)S(1)}, f32[2048]{0:T(1024)}, u32[]{:S(2)}) copy-start(f32[2048]{0:T(1024)} %param.25) | copy-start | bytes 24580
  260.1 201.8 %all-gather.17.cloned.1.call-start = ((), (), s32[]{:S(2)}) async-start(), calls=%async_computation.7 | async-start | bytes 17825792 | tf_op jit(solution)/shard_map/all_gather | solution.py:127
  260.7 451.2 %all-gather.19.cloned.1.call-start = ((), (), s32[]{:S(2)}) async-start(), calls=%async_computation.8 | async-start | bytes 17825792 | tf_op jit(solution)/shard_map/all_gather | solution.py:133
  261.4 472.1 %reduce-scatter.5.cloned.1.call-start = ((), (), s32[]{:S(2)}) async-start(), calls=%async_computation.9 | async-start | bytes 1179648 | tf_op jit(solution)/shard_map/reduce_scatter | solution.py:136
  271.9 461.6 %copy-start.7 = (bf16[96,2048]{1,0:T(8,128)(2,1)S(1)}, bf16[96,2048]{1,0:T(8,128)(2,1)}, u32[]{:S(2)}) copy-start(bf16[96,2048]{1,0:T(8,128)(2,1)} %reduce-scatter.3.cloned.1.call-done) | copy-start | bytes 1179652
  711.9 23.5 %copy-start.1 = (bf16[256,2048]{1,0:T(8,128)(2,1)S(1)}, bf16[256,2048]{1,0:T(8,128)(2,1)}, u32[]{:S(2)}) copy-start(bf16[256,2048]{1,0:T(8,128)(2,1)} %param.23) | copy-start | bytes 3145732
Sparse Core Ops, SparseCore 0:
  10.1 60.9 all-gather.8
  73.8 56.6 all-gather.12
  133.3 56.6 all-gather.10
  192.7 56.7 all-gather.14
  260.2 6.8 reduce-scatter.2
  269.8 192.1 all-gather.16
  464.6 247.2 all-gather.18
  727.2 6.3 reduce-scatter.4
where the time goes:
time: 743 us; the launch traced here: 742 us
  waiting for transfers between devices  557 us (75%)
  blocking collectives  82.2 us (11%)
  matrix products  51.1 us (7%)
  local copies, waits for them, and re-layouts  21.5 us (3%)
  other arithmetic  16.1 us (2%)
  between operations  13.7 us (2%)
    all_gather x1, waiting for transfers between devices, local(): lax.all_gather(down_weight, 'sp', axis=1, tiled=True)  250 us
    all_gather x1, waiting for transfers between devices, local(): lax.all_gather(up_weight, 'sp', axis=0, tiled=True)  190 us
    all_gather x1, waiting for transfers between devices, local(): lax.all_gather(values_narrow, 'sp', axis=0, tiled=True)  48.9 us
    all_gather x1, blocking collectives, local(): lax.all_gather(gates_narrow, 'sp', axis=0, tiled=True)  43.5 us
    all_gather x1, waiting for transfers between devices, local(): piece_values_broad = lax.all_gather(values_broad, 'sp', axis=0, tiled=True)  42.1 us
    all_gather x1, blocking collectives, local(): lax.all_gather(gates_broad, 'sp', axis=0, tiled=True)  36.3 us
    dot_general x2, matrix products, group_update(): jnp.einsum('hqk,khd->hqd', weights.astype(jnp.bfloat16), values.reshape(k...  17.7 us
    dot_general x2, matrix products, group_update(): jnp.einsum('qhd,khd->hqk', queries.reshape(query_count, heads, head_size)...  15.4 us
  transfers between devices with their start and end apart: 8, of which 7 were waited for; matrix products, arithmetic and copies ran while one was open for 7% of the time, Pallas kernels for 0%

commit v1 on v0

--- a/solution.py
+++ b/solution.py
@@ -1,3 +1,4 @@
+import functools
 import jax
 import jax.numpy as jnp
 from jax import lax
@@ -5,6 +6,14 @@
 
 A_DIM = 32
 B_DIM = 64
+
+
+def _fill_positions(original, a_name):
+    row_out = jax.lax.all_gather(original, a_name)
+    return jnp.concatenate(row_out, axis=1)
+
+
+bring_the_boxes = functools.partial(_fill_positions, a_name="sp")
 
 
 def group_update(state, queries, keys, values, query_gates, key_gates, allowed, head_size):
@@ -128,11 +137,7 @@
         preferred_element_type=jnp.float32,
     )
     hidden = jnp.square(jax.nn.relu(up_total)).astype(jnp.bfloat16)
-    down_term = jnp.dot(
-        hidden,
-        lax.all_gather(down_weight, "sp", axis=1, tiled=True),
-        preferred_element_type=jnp.float32,
-    )
+    down_term = jnp.dot(hidden, bring_the_boxes(down_weight), preferred_element_type=jnp.float32)
     summed_rows = lax.psum_scatter(
         down_term.astype(jnp.bfloat16), "tp", scatter_dimension=0, tiled=True
     ).astype(jnp.float32)

time: 743 us -> 686 us (0.923)
  waiting for transfers between devices: 557 us -> 478 us
  local copies, waits for them, and re-layouts: 21.5 us -> 42.8 us
    all_gather x1, waiting for transfers between devices: 250 us -> 190 us  [_fill_positions(): row_out = jax.lax.all_gather(original, a_name)]
    reshape x0 -> x1, local copies, waits for them, and re-layouts: none -> 21.3 us  [_fill_positions(): return jnp.concatenate(row_out, axis=1)]
    all_gather x1, waiting for transfers between devices: 190 us -> 171 us  [local(): lax.all_gather(up_weight, 'sp', axis=0, tiled=True)]
  transfers between devices with their start and end apart: 8 -> 8, of which waited for: 7 -> 7; matrix products, arithmetic and copies ran while one was open for 7% -> 11% of each run, Pallas kernels for 0% -> 0%
where the time goes in v1:
time: 686 us; the launch traced here: 685 us
  waiting for transfers between devices  478 us (70%)
  blocking collectives  82.2 us (12%)
  matrix products  52.2 us (8%)
  local copies, waits for them, and re-layouts  42.8 us (6%)
  other arithmetic  16.1 us (2%)
  between operations  13.7 us (2%)
    all_gather x1, waiting for transfers between devices, _fill_positions(): row_out = jax.lax.all_gather(original, a_name)  190 us
    all_gather x1, waiting for transfers between devices, local(): lax.all_gather(up_weight, 'sp', axis=0, tiled=True)  171 us
    all_gather x1, waiting for transfers between devices, local(): lax.all_gather(values_narrow, 'sp', axis=0, tiled=True)  48.9 us
    all_gather x1, blocking collectives, local(): lax.all_gather(gates_narrow, 'sp', axis=0, tiled=True)  43.5 us
    all_gather x1, waiting for transfers between devices, local(): piece_values_broad = lax.all_gather(values_broad, 'sp', axis=0, tiled=True)  42.1 us
    all_gather x1, blocking collectives, local(): lax.all_gather(gates_broad, 'sp', axis=0, tiled=True)  36.3 us
    reshape x1, local copies, waits for them, and re-layouts, _fill_positions(): return jnp.concatenate(row_out, axis=1)  21.3 us
    dot_general x2, matrix products, group_update(): jnp.einsum('hqk,khd->hqd', weights.astype(jnp.bfloat16), values.reshape(k...  17.7 us
  transfers between devices with their start and end apart: 8, of which 7 were waited for; matrix products, arithmetic and copies ran while one was open for 11% of the time, Pallas kernels for 0%

profile of v1, /device:TPU:0, one launch (start us, length us, event | category | flops | bytes accessed | tf_op | source)
XLA Modules:
  0.0 685.4 jit_solution(3921579949885772902)
XLA Ops:
  6.5 0.7 all-gather.10.cloned.1.call-update
  7.3 0.0 all-gather.14.cloned.1.call-start
  7.3 0.7 all-gather.14.cloned.1.call-update
  8.0 0.0 all-gather.12.cloned.1.call-start
  8.1 0.7 all-gather.12.cloned.1.call-update
  8.7 0.0 all-gather.16.cloned.1.call-start
  8.8 0.5 all-gather.16.cloned.1.call-update
  9.3 0.0 reduce-scatter.3.cloned.1.call-start
  9.4 1.3 iota_compare_fusion
  10.7 43.5 %all-gather.1 = f32[16,192,8]{1,2,0:T(8,128)S(1)} all-gather(f32[1,192,8]{1,2,0:T(8,128)} %bitcast.65), channel_id=1, replica_groups=mesh['sp'=16,'tp'=2] {'sp'}, dimensions={0}, use_global_device_ids=true | all-gather | bytes 104448 | tf_op jit(solution)/shard_map/all_gather | solution.py:86
  54.3 0.7 reshape.101
  55.0 1.7 copy.38
  56.7 36.3 %all-gather.2 = f32[16,192,4]{1,2,0:T(4,128)S(1)} all-gather(f32[1,192,4]{1,2,0:T(4,128)} %bitcast.71), channel_id=1, replica_groups=mesh['sp'=16,'tp'=2] {'sp'}, dimensions={0}, use_global_device_ids=true | all-gather | bytes 52224 | tf_op jit(solution)/shard_map/all_gather | solution.py:87
  93.0 0.1 reshape.103
  93.1 1.6 copy.42
  94.7 2.6 copy.39
  97.3 7.4 %fusion.2 = (f32[8,192]{1,0:T(8,128)S(1)}, f32[8,192,3072]{2,1,0:T(8,128)S(1)}) fusion(f32[8,3072]{1,0:T(8,128)} %bitcast.58, f32[8,192]{1,0:T(8,128)} %bitcast.66, pred[192,3072]{1,0:T(8,128)(4,1)} %get-tuple-element.5, bf16[192,8,32]{0,2,1:T(8,128)(2,1)} %bitcast.62, bf16[3072,8,32]{0,2,1:T(8,128)(2,1)} %bitcast.56), kind=kOutput, calls=%fused_computation.4 | convolution fusion | flops 325581312 | bytes 21245952 | tf_op jit(solution)/shard_map/qhd,khd->hqk/dot_general | solution.py:24
  104.8 6.4 copy-done.4
  111.2 0.4 copy-done.14
  111.5 8.6 %fusion = f32[8,192]{1,0:T(8,128)} fusion(f32[8,192,3072]{2,1,0:T(8,128)S(1)} %get-tuple-element.8, f32[192,3072]{1,0:T(8,128)S(1)} %get-tuple-element.6, f32[8,192]{1,0:T(8,128)S(1)} %broadcast_maximum_fusion, f32[8,3072]{1,0:T(8,128)S(1)} %bitcast.59, f32[8,192]{1,0:T(8,128)S(1)} %bitcast.67, pred[192,3072]{1,0:T(8,128)(4,1)S(1)} %copy-done.8), kind=kLoop, calls=%fused_computation.2 | loop fusion | flops 33028608 | bytes 21940224 | tf_op jit(solution)/shard_map/reduce_sum | solution.py:34
  120.2 10.4 %all-gather.14.cloned.1.call-done = bf16[3072,256]{1,0:T(8,128)(2,1)} async-done(((bf16[192,256]{1,0:T(8,128)(2,1)}), bf16[3072,256]{1,0:T(8,128)(2,1)}) %all-gather.14.cloned.1.call-update) | async-done | bytes 1572880 | tf_op jit(solution)/shard_map/all_gather | solution.py:96
  130.6 2.6 copy.43
  133.2 8.0 %fusion.41 = (f32[4,192]{1,0:T(4,128)S(1)}, f32[4,192,3072]{2,1,0:T(8,128)}) fusion(f32[4,3072]{1,0:T(4,128)S(1)} %bitcast.64, f32[4,192]{1,0:T(4,128)} %bitcast.72, bf16[192,4,64]{0,2,1:T(8,128)(2,1)} %bitcast.61, bf16[3072,4,64]{0,2,1:T(8,128)(2,1)} %bitcast.55, pred[192,3072]{1,0:T(8,128)(4,1)} %get-tuple-element.5), kind=kOutput, calls=%fused_computation.43 | convolution fusion | flops 313785600 | bytes 11753472 | tf_op jit(solution)/shard_map/qhd,khd->hqk/dot_general | solution.py:24
  141.1 48.9 %all-gather.12.cloned.1.call-done = bf16[3072,256]{1,0:T(8,128)(2,1)} async-done(((bf16[192,256]{1,0:T(8,128)(2,1)}), bf16[3072,256]{1,0:T(8,128)(2,1)}) %all-gather.12.cloned.1.call-update) | async-done | bytes 1572880 | tf_op jit(solution)/shard_map/all_gather | solution.py:95
  190.1 2.7 copy.41
  192.8 11.0 %fusion.24 = bf16[192,8,32]{0,2,1:T(8,128)(2,1)S(1)} fusion(bf16[3072,8,32]{0,2,1:T(8,128)(2,1)} %bitcast.54, f32[8,192,3072]{2,1,0:T(8,128)} %copy-done.4, f32[192,3072]{1,0:T(8,128)} %copy-done.2, f32[8,192]{1,0:T(8,128)S(1)} %copy-done.15, f32[8,3072]{1,0:T(8,128)S(1)} %bitcast.60, f32[8,192]{1,0:T(8,128)S(1)} %bitcast.68, ...), kind=kOutput, calls=%fused_computation.27 | convolution fusion | flops 335118336 | bytes 23611392 | tf_op jit(solution)/shard_map/hqk,khd->hqd/dot_general | solution.py:35
  203.8 1.6 fusion.42
  205.4 1.8 fusion.6
  207.3 42.1 %all-gather.16.cloned.1.call-done = bf16[3072,256]{1,0:T(8,128)(2,1)} async-done(((bf16[192,256]{1,0:T(8,128)(2,1)}), bf16[3072,256]{1,0:T(8,128)(2,1)}) %all-gather.16.cloned.1.call-update) | async-done | bytes 1572880 | tf_op jit(solution)/shard_map/all_gather | solution.py:97
  249.4 2.6 copy.45
  252.0 6.7 fusion.30
  258.8 1.3 fusion.14
  260.1 0.0 reduce-scatter.3.cloned.1.call-update
  260.1 0.0 all-gather.20.cloned.1.call-start
  260.2 0.5 all-gather.20.cloned.1.call-update
  260.7 0.0 all-gather.18.cloned.1.call-start
  260.7 0.7 all-gather.18.cloned.1.call-update
  261.4 0.0 reduce-scatter.5.cloned.1.call-start
  261.5 5.7 reduce-scatter.3.cloned.1.call-done
  267.1 1.2 fusion.33
  268.4 1.2 fusion.35
  269.6 2.4 all_gather.36
  271.9 190.0 %all-gather.20.cloned.1.call-done = bf16[65536,128]{1,0:T(8,128)(2,1)} async-done(((bf16[4096,128]{1,0:T(8,128)(2,1)}), bf16[65536,128]{1,0:T(8,128)(2,1)}) %all-gather.20.cloned.1.call-update) | async-done | bytes 16777232 | tf_op jit(solution)/shard_map/all_gather | solution.py:12
  461.9 21.3 %copy.46 = bf16[4096,16,128]{0,2,1:T(8,128)(2,1)} copy(bf16[4096,16,128]{2,0,1:T(8,128)(2,1)} %bitcast.51) | data formatting | bytes 33554432 | tf_op jit(solution)/shard_map/reshape | solution.py:13
  483.2 170.7 %all-gather.18.cloned.1.call-done = bf16[2048,4096]{1,0:T(8,128)(2,1)} async-done(((bf16[128,4096]{1,0:T(8,128)(2,1)}), bf16[2048,4096]{1,0:T(8,128)(2,1)}) %all-gather.18.cloned.1.call-update) | async-done | bytes 16777232 | tf_op jit(solution)/shard_map/all_gather | solution.py:136
  653.9 16.2 %convolution_convert_fusion = bf16[192,2048]{1,0:T(8,128)(2,1)} fusion(bf16[4096,2048]{0,1:T(8,128)(2,1)} %bitcast.52, bf16[192,2048]{1,0:T(8,128)(2,1)S(1)} %all_gather.36, bf16[2048,4096]{1,0:T(8,128)(2,1)} %all-gather.18.cloned.1.call-done), kind=kOutput, calls=%fused_computation.18 | convolution fusion | flops 6445203456 | bytes 35127296 | tf_op jit(solution)/shard_map/dot_general | solution.py:140
  670.1 6.5 reduce-scatter.5.cloned.1.call-done
  676.6 1.9 fusion.36
  (50 shorter events, 0.2 us)
Async XLA Ops:
  6.5 197.3 %copy-start = (bf16[256,2048]{1,0:T(8,128)(2,1)S(1)}, bf16[256,2048]{1,0:T(8,128)(2,1)}, u32[]{:S(2)}) copy-start(bf16[256,2048]{1,0:T(8,128)(2,1)} %param.23) | copy-start | bytes 3145732
  6.5 88.2 %all-gather.10.cloned.1.call-start = ((), (), s32[]{:S(2)}) async-start(), calls=%async_computation.2 | async-start | bytes 1671168 | tf_op jit(solution)/shard_map/all_gather | solution.py:94
  7.3 123.3 %all-gather.14.cloned.1.call-start = ((), (), s32[]{:S(2)}) async-start(), calls=%async_computation.4 | async-start | bytes 1671168 | tf_op jit(solution)/shard_map/all_gather | solution.py:96
  8.0 182.0 %all-gather.12.cloned.1.call-start = ((), (), s32[]{:S(2)}) async-start(), calls=%async_computation.3 | async-start | bytes 1671168 | tf_op jit(solution)/shard_map/all_gather | solution.py:95
  8.7 240.7 %all-gather.16.cloned.1.call-start = ((), (), s32[]{:S(2)}) async-start(), calls=%async_computation.5 | async-start | bytes 1671168 | tf_op jit(solution)/shard_map/all_gather | solution.py:97
  9.3 257.8 %reduce-scatter.3.cloned.1.call-start = ((), (), s32[]{:S(2)}) async-start(), calls=%async_computation.6 | async-start | bytes 1179648 | tf_op jit(solution)/shard_map/reduce_scatter | solution.py:123
  10.7 94.0 %copy-start.2 = (f32[192,3072]{1,0:T(8,128)}, f32[192,3072]{1,0:T(8,128)S(1)}, u32[]{:S(2)}) copy-start(f32[192,3072]{1,0:T(8,128)S(1)} %get-tuple-element.6) | copy-start | bytes 7077892
  97.3 14.2 %copy-start.8 = (pred[192,3072]{1,0:T(8,128)(4,1)S(1)}, pred[192,3072]{1,0:T(8,128)(4,1)}, u32[]{:S(2)}) copy-start(pred[192,3072]{1,0:T(8,128)(4,1)} %get-tuple-element.5) | copy-start | bytes 1769476
  97.3 14.2 %copy-start.11 = (f32[3072,8]{0,1:T(8,128)S(1)}, f32[3072,8]{0,1:T(8,128)}, u32[]{:S(2)}) copy-start(f32[3072,8]{0,1:T(8,128)} %reshape.101) | copy-start | bytes 294916
  97.3 14.2 %copy-start.12 = (f32[192,8]{0,1:T(8,128)S(1)}, f32[192,8]{0,1:T(8,128)}, u32[]{:S(2)}) copy-start(f32[192,8]{0,1:T(8,128)} %param.21) | copy-start | bytes 18436
  104.7 6.4 copy-start.4
  104.7 6.8 copy-start.14
  133.2 59.6 %copy-start.9 = (pred[192,3072]{1,0:T(8,128)(4,1)S(1)}, pred[192,3072]{1,0:T(8,128)(4,1)}, u32[]{:S(2)}) copy-start(pred[192,3072]{1,0:T(8,128)(4,1)} %get-tuple-element.5) | copy-start | bytes 1769476
  133.2 59.6 %copy-start.13 = (f32[192,8]{0,1:T(8,128)S(1)}, f32[192,8]{0,1:T(8,128)}, u32[]{:S(2)}) copy-start(f32[192,8]{0,1:T(8,128)} %param.21) | copy-start | bytes 18436
  133.2 59.6 %copy-start.15 = (f32[8,192]{1,0:T(8,128)S(1)}, f32[8,192]{1,0:T(8,128)}, u32[]{:S(2)}) copy-start(f32[8,192]{1,0:T(8,128)} %copy-done.14) | copy-start | bytes 18436
  133.2 59.6 %copy-start.17 = (f32[8,192]{1,0:T(8,128)S(1)}, f32[8,192]{1,0:T(8,128)}, u32[]{:S(2)}) copy-start(f32[8,192]{1,0:T(8,128)} %fusion) | copy-start | bytes 18436
  190.0 15.4 %slice-start = ((s8[9437184]{0:T(1024)(128)(4,1)}), s8[1048576]{0:T(1024)(128)(4,1)S(1)}, s32[]{:S(2)}) async-start(s8[9437184]{0:T(1024)(128)(4,1)} %bitcast.49), calls=%async_computation.10 | async-start | bytes 2097152
  192.8 12.6 %slice-start.1 = ((s8[9437184]{0:T(1024)(128)(4,1)}), s8[4194304]{0:T(1024)(128)(4,1)S(1)}, s32[]{:S(2)}) async-start(s8[9437184]{0:T(1024)(128)(4,1)} %bitcast.49), calls=%async_computation.11 | async-start | bytes 8388608
  192.8 12.6 %slice-start.2 = ((s8[9437184]{0:T(1024)(128)(4,1)}), s8[4194304]{0:T(1024)(128)(4,1)S(1)}, s32[]{:S(2)}) async-start(s8[9437184]{0:T(1024)(128)(4,1)} %bitcast.49), calls=%async_computation.12 | async-start | bytes 8388608
  192.8 12.6 %copy-start.3 = (f32[192,3072]{1,0:T(8,128)S(1)}, f32[192,3072]{1,0:T(8,128)}, u32[]{:S(2)}) copy-start(f32[192,3072]{1,0:T(8,128)} %copy-done.2) | copy-start | bytes 7077892
  207.3 51.5 %copy-start.5 = (f32[192,2048]{1,0:T(8,128)S(1)}, f32[192,2048]{1,0:T(8,128)}, u32[]{:S(2)}) copy-start(f32[192,2048]{1,0:T(8,128)} %fusion.42) | copy-start | bytes 4718596
  207.3 51.5 %copy-start.10 = (bf16[256,2048]{1,0:T(8,128)(2,1)S(1)}, bf16[256,2048]{1,0:T(8,128)(2,1)}, u32[]{:S(2)}) copy-start(bf16[256,2048]{1,0:T(8,128)(2,1)} %param.24) | copy-start | bytes 3145732
  252.0 15.1 %copy-start.6 = (bf16[96,2048]{1,0:T(8,128)(2,1)S(1)}, bf16[96,2048]{1,0:T(8,128)(2,1)}, u32[]{:S(2)}) copy-start(bf16[96,2048]{1,0:T(8,128)(2,1)} %param.14) | copy-start | bytes 1179652
  252.0 16.4 %copy-start.16 = (f32[2048]{0:T(1024)S(1)}, f32[2048]{0:T(1024)}, u32[]{:S(2)}) copy-start(f32[2048]{0:T(1024)} %param.25) | copy-start | bytes 24580
  260.1 201.8 %all-gather.20.cloned.1.call-start = ((), (), s32[]{:S(2)}) async-start(), calls=%async_computation.9 | async-start | bytes 17825792 | tf_op jit(solution)/shard_map/all_gather | solution.py:12
  260.7 393.2 %all-gather.18.cloned.1.call-start = ((), (), s32[]{:S(2)}) async-start(), calls=%async_computation.7 | async-start | bytes 17825792 | tf_op jit(solution)/shard_map/all_gather | solution.py:136
  261.4 415.2 %reduce-scatter.5.cloned.1.call-start = ((), (), s32[]{:S(2)}) async-start(), calls=%async_computation.8 | async-start | bytes 1179648 | tf_op jit(solution)/shard_map/reduce_scatter | solution.py:141
  653.9 22.7 %copy-start.7 = (bf16[96,2048]{1,0:T(8,128)(2,1)S(1)}, bf16[96,2048]{1,0:T(8,128)(2,1)}, u32[]{:S(2)}) copy-start(bf16[96,2048]{1,0:T(8,128)(2,1)} %reduce-scatter.3.cloned.1.call-done) | copy-start | bytes 1179652
  653.9 24.6 %copy-start.1 = (bf16[256,2048]{1,0:T(8,128)(2,1)S(1)}, bf16[256,2048]{1,0:T(8,128)(2,1)}, u32[]{:S(2)}) copy-start(bf16[256,2048]{1,0:T(8,128)(2,1)} %param.23) | copy-start | bytes 3145732
Sparse Core Ops, SparseCore 0:
  10.1 60.9 all-gather.9
  73.8 56.6 all-gather.13
  133.3 56.6 all-gather.11
  192.7 56.7 all-gather.15
  260.2 6.8 reduce-scatter.2
  269.8 192.1 all-gather.19
  464.7 189.1 all-gather.17
  670.3 6.3 reduce-scatter.4
